TPU v7x, 128 devices: a whole 4x4x4 slice. The times are simulated.
128 devices in a mesh: fs: 16 (over z, y), rep: 4 (over x), tp: 2 (over core).
Axes of the slice: x: 4, y: 4, z: 4, core: 2. Of those that a mesh axis runs over, the one named last changes fastest.
Arguments:
- query_input: bfloat16 [65536, 4096], P(('fs', 'rep')), may hold values from -6 to 6
- query_cotangent: bfloat16 [65536, 1024], P(('fs', 'rep'), 'tp'), may hold values from -0.0234375 to 0.0234375
- branch_output: bfloat16 [65536, 2048], P(('fs', 'rep')), may hold values from -6 to 6
- layer_cotangent: bfloat16 [65536, 4096], P(('fs', 'rep'), 'tp'), may hold values from -0.0234375 to 0.0234375
- query_weight: float32 [4096, 1024], P(('rep', 'fs'), 'tp'), may hold values from -0.09375 to 0.09375
- output_weight: float32 [2048, 4096], P(('rep', 'fs'), 'tp'), may hold values from -0.125 to 0.125
- query_basis: bfloat16 [4096, 512], P(('rep', 'fs')), may hold values from -0.09375 to 0.09375
- output_basis: bfloat16 [2048, 512], P(('rep', 'fs')), may hold values from -0.125 to 0.125
- query_first: float32 [512, 1024], P(('rep', 'fs'), 'tp'), may hold values from -20 to 20
- query_second: float32 [512, 1024], P(('rep', 'fs'), 'tp'), may hold values from 0.25 to 2
- output_first: float32 [512, 4096], P(('rep', 'fs'), 'tp'), may hold values from -20 to 20
- output_second: float32 [512, 4096], P(('rep', 'fs'), 'tp'), may hold values from 0.25 to 2
Outputs:
- query_update: float32 [4096, 1024], P(('rep', 'fs'), 'tp')
- output_update: float32 [2048, 4096], P(('rep', 'fs'), 'tp')
- query_first_next: float32 [512, 1024], P(('rep', 'fs'), 'tp')
- query_second_next: float32 [512, 1024], P(('rep', 'fs'), 'tp')
- output_first_next: float32 [512, 4096], P(('rep', 'fs'), 'tp')
- output_second_next: float32 [512, 4096], P(('rep', 'fs'), 'tp')
- query_copy: bfloat16 [4096, 1024], P('rep', 'tp')
- output_copy: bfloat16 [2048, 4096], P('rep', 'tp')
All inputs are finite; a program needn't handle non-finite values.
Results may differ from a plain program's by a relative error of at most 0.0055.
Values may be sent and summed in bfloat16 or wider, within the bound.
A program may use at most 128 MiB of HBM per device.

v0:
```python
import jax
import jax.numpy as jnp
from jax import lax
from jax.sharding import Mesh
from jax.sharding import PartitionSpec as P

D = 4096
QKW = 1024
R = 512
REP_FS = ("rep", "fs_0", "fs_1")
FS_REP_TP = ("fs_0", "fs_1", "rep", "tp")
FS = ("fs_0", "fs_1")
FS_REP = ("fs_0", "fs_1", "rep")


beta_first = 0.6
beta_second = 0.8
step_rate = 0.01
small_eps = 1e-06


def joined_along(tiles, dim):
    tiles = jnp.moveaxis(tiles, 0, dim)
    shape = tiles.shape
    return tiles.reshape(*shape[:dim], shape[dim] * shape[dim + 1], *shape[dim + 2 :])


def gather_together(arrays, axis, dims):
    ravelled = jnp.concatenate([a.reshape(-1) for a in arrays])
    lines, at, gathered = (lax.all_gather(ravelled, axis), 0, [])
    for a, dim in zip(arrays, dims):
        tiles = lines[:, at : at + a.size].reshape(-1, *a.shape)
        gathered.append(joined_along(tiles, dim))
        at += a.size
    return tuple(gathered)


def in_blocks(value, dim, count):
    shape = value.shape
    tiles = value.reshape(*shape[:dim], count, shape[dim] // count, *shape[dim + 1 :])
    return jnp.moveaxis(tiles, dim, 0)


def summed_on_arrival(value, axis, dim):
    count = lax.axis_size(axis)
    tiles = lax.all_to_all(in_blocks(value, dim, count), axis, 0, 0, tiled=True)
    return jnp.sum(tiles.astype(jnp.float32), axis=0)


def over_axes(value, axes):
    for axis in axes:
        value = lax.psum(value, axis)
    return value


def sent_together(arrays, axis, dim, along):
    both = jnp.concatenate(arrays, axis=along)
    whole, at, gathered = (lax.all_gather(both, axis, axis=dim, tiled=True), 0, [])
    for a in arrays:
        gathered.append(lax.slice_in_dim(whole, at, at + a.shape[along], axis=along))
        at += a.shape[along]
    return tuple(gathered)


def split_parts(values):
    upper = values.astype(jnp.bfloat16)
    lower = (values - upper.astype(jnp.float32)).astype(jnp.bfloat16)
    return (upper, lower)


def split_rows(inner, cotangent):
    upper, lower = split_parts(inner)
    dims = (((0,), (0,)), ((), ()))
    return lax.dot_general(
        upper, cotangent, dims, preferred_element_type=jnp.float32
    ) + lax.dot_general(lower, cotangent, dims, preferred_element_type=jnp.float32)


def moments(first, second, projected):
    first_next = beta_first * first + (1.0 - beta_first) * projected
    second_next = beta_second * second + (1.0 - beta_second) * projected * projected
    return (first_next, second_next, first_next / jnp.sqrt(second_next))


def body(
    query_input,
    query_cotangent,
    branch_output,
    layer_cotangent,
    query_weight,
    output_weight,
    query_basis,
    output_basis,
    query_first,
    query_second,
    output_first,
    output_second,
):
    query_whole, output_whole = gather_together((query_basis, output_basis), REP_FS, (0, 0))
    query_inner = jnp.dot(query_input, query_whole, preferred_element_type=jnp.float32)
    output_inner = jnp.dot(branch_output, output_whole, preferred_element_type=jnp.float32)
    projected_q = summed_on_arrival(
        split_rows(query_inner, query_cotangent).astype(jnp.bfloat16), REP_FS, 0
    )
    projected_o = summed_on_arrival(
        split_rows(output_inner, layer_cotangent).astype(jnp.bfloat16), REP_FS, 0
    )
    first_q, second_q, normed_q = moments(query_first, query_second, projected_q)
    first_o, second_o, normed_o = moments(output_first, output_second, projected_o)
    totals = (
        over_axes(jnp.sum(normed_q * normed_q), FS_REP_TP),
        over_axes(jnp.sum(normed_o * normed_o), FS_REP_TP),
    )
    scale_q = lax.rsqrt(totals[0] / (R * QKW) + small_eps)
    scale_o = lax.rsqrt(totals[1] / (R * D) + small_eps)
    pieces = sent_together(
        (normed_q.astype(jnp.bfloat16), normed_o.astype(jnp.bfloat16)), REP_FS, 0, 1
    )
    summed_q = jnp.dot(query_basis, pieces[0], preferred_element_type=jnp.float32)
    summed_o = jnp.dot(output_basis, pieces[1], preferred_element_type=jnp.float32)
    update_q = scale_q * summed_q
    update_o = scale_o * summed_o
    query_copy, output_copy = gather_together(
        (
            (query_weight - step_rate * update_q).astype(jnp.bfloat16),
            (output_weight - step_rate * update_o).astype(jnp.bfloat16),
        ),
        FS,
        (0, 0),
    )
    return (update_q, update_o, first_q, second_q, first_o, second_o, query_copy, output_copy)


def solution(mesh):
    split = Mesh(
        mesh.devices.reshape(4, 4, mesh.shape["rep"], mesh.shape["tp"]),
        ("fs_0", "fs_1", "rep", "tp"),
    )
    return jax.shard_map(
        body,
        mesh=split,
        in_specs=(
            P(FS_REP, None),
            P(FS_REP, "tp"),
            P(FS_REP, None),
            P(FS_REP, "tp"),
            P(REP_FS, "tp"),
            P(REP_FS, "tp"),
            P(REP_FS, None),
            P(REP_FS, None),
            P(REP_FS, "tp"),
            P(REP_FS, "tp"),
            P(REP_FS, "tp"),
            P(REP_FS, "tp"),
        ),
        out_specs=(
            P(REP_FS, "tp"),
            P(REP_FS, "tp"),
            P(REP_FS, "tp"),
            P(REP_FS, "tp"),
            P(REP_FS, "tp"),
            P(REP_FS, "tp"),
            P("rep", "tp"),
            P("rep", "tp"),
        ),
        check_vma=False,
    )
```

profile of v0, /device:TPU:1, one launch (start us, length us, event | category | flops | bytes accessed | tf_op | source)
XLA Modules:
  0.0 311.2 jit_solution(834793160532769381)
XLA Ops:
  9.6 76.4 %all-gather.8.cloned.1.call-done = bf16[3145728]{0:T(1024)(128)(2,1)} async-done(((bf16[49152]{0:T(1024)(128)(2,1)}), bf16[3145728]{0:T(1024)(128)(2,1)}) %all-gather.8.cloned.1.call-update) | async-done | bytes 6291472 | tf_op jit(solution)/shard_map/all_gather | solution.py:30
  86.1 8.9 %reshape.40 = bf16[64,49152]{1,0:T(8,128)(2,1)} reshape(bf16[3145728]{0:T(1024)(128)(2,1)} %all-gather.8.cloned.1.call-done) | data formatting | bytes 12582912 | tf_op jit(solution)/shard_map/all_gather | solution.py:30
  94.9 4.5 %slice.24 = bf16[64,32768]{1,0:T(8,128)(2,1)} slice(bf16[64,49152]{1,0:T(8,128)(2,1)} %reshape.40), slice={[0:64], [0:32768]} | slice | bytes 8388608 | tf_op jit(solution)/shard_map/slice | solution.py:32
  99.5 7.6 %reshape_reshape.12 = bf16[4096,512]{1,0:T(8,128)(2,1)} reshape(bf16[64,32768]{1,0:T(8,128)(2,1)} %slice.24) | data formatting | bytes 8388608 | tf_op jit(solution)/shard_map/reshape;reshape | solution.py:25
  107.1 2.3 reshape_reshape.13
  109.4 8.2 %fusion.29 = f32[512,1024]{1,0:T(8,128)S(1)} fusion(bf16[4096,512]{1,0:T(8,128)(2,1)} %reshape_reshape.12, bf16[1024,4096]{1,0:T(8,128)(2,1)} %param.12), kind=kOutput, calls=%fused_computation.44 | convolution fusion | flops 4294967296 | bytes 14680064 | tf_op jit(solution)/shard_map/dot_general | solution.py:100
  119.9 8.3 %all-to-all-start = ((bf16[64,8,512]{2,1,0:T(8,128)(2,1)}), bf16[64,8,512]{2,1,0:T(8,128)(2,1)S(1)}, u32[]{:S(2)}, u32[]{:S(2)}) async-start(bf16[64,8,512]{2,1,0:T(8,128)(2,1)} %fusion.6), calls=%async_computation | async-start | bytes 1048576 | tf_op jit(solution)/shard_map/all_to_all | solution.py:46
  128.2 4.7 %fusion.30 = f32[512,1024]{1,0:T(8,128)S(1)} fusion(bf16[2048,512]{1,0:T(8,128)(2,1)S(1)} %copy-done.2, bf16[1024,2048]{1,0:T(8,128)(2,1)} %param.14), kind=kOutput, calls=%fused_computation.45 | convolution fusion | flops 2147483648 | bytes 8388608 | tf_op jit(solution)/shard_map/dot_general | solution.py:101
  133.0 2.3 fusion.23
  135.3 3.7 %fusion = bf16[64,8,2048]{2,1,0:T(8,128)(2,1)} fusion(f32[512,2048]{1,0:T(8,128)S(1)} %fusion.23, bf16[1024,2048]{1,0:T(8,128)(2,1)S(1)} %copy-done.17, f32[512,1024]{1,0:T(8,128)S(1)} %fusion.30), kind=kOutput, calls=%fused_computation.2 | convolution fusion | flops 2151677952 | bytes 12582912 | tf_op jit(solution)/shard_map/dot_general | solution.py:76
  139.8 9.3 %all-to-all-start.1 = ((bf16[64,8,2048]{2,1,0:T(8,128)(2,1)}), bf16[64,8,2048]{2,1,0:T(8,128)(2,1)S(1)}, u32[]{:S(2)}, u32[]{:S(2)}) async-start(bf16[64,8,2048]{2,1,0:T(8,128)(2,1)} %fusion), calls=%async_computation.1 | async-start | bytes 4194304 | tf_op jit(solution)/shard_map/all_to_all | solution.py:46
  149.9 26.2 %all-to-all-done.1 = bf16[64,8,2048]{2,1,0:T(8,128)(2,1)S(1)} async-done(((bf16[64,8,2048]{2,1,0:T(8,128)(2,1)}), bf16[64,8,2048]{2,1,0:T(8,128)(2,1)S(1)}, u32[]{:S(2)}, u32[]{:S(2)}) %all-to-all-start.1) | async-done | bytes 2097184 | tf_op jit(solution)/shard_map/all_to_all | solution.py:46
  177.8 8.6 %all-reduce.2 = (f32[]{:T(128)}, f32[]{:T(128)}) all-reduce(f32[]{:T(128)} %get-tuple-element.19, f32[]{:T(128)} %get-tuple-element.16), channel_id=1, replica_groups=mesh['fs_0'=4,'fs_1'=4,'rep'=4,'tp'=2] {'fs_0'}, use_global_device_ids=true, to_apply=%region_2.0 | all-reduce | flops 2 | bytes 16 | tf_op jit(solution)/shard_map/psum | solution.py:52
  186.4 7.5 %all-reduce.1 = (f32[]{:T(128)}, f32[]{:T(128)}) all-reduce(f32[]{:T(128)} %get-tuple-element.12, f32[]{:T(128)} %get-tuple-element.13), channel_id=1, replica_groups=mesh['fs_0'=4,'fs_1'=4,'rep'=4,'tp'=2] {'fs_1'}, use_global_device_ids=true, to_apply=%region_3.0 | all-reduce | flops 2 | bytes 16 | tf_op jit(solution)/shard_map/psum | solution.py:52
  194.0 9.8 %all-reduce = (f32[]{:T(128)}, f32[]{:T(128)}) all-reduce(f32[]{:T(128)} %get-tuple-element.10, f32[]{:T(128)} %get-tuple-element.11), channel_id=1, replica_groups=mesh['fs_0'=4,'fs_1'=4,'rep'=4,'tp'=2] {'rep'}, use_global_device_ids=true, to_apply=%region_4.0 | all-reduce | flops 2 | bytes 16 | tf_op jit(solution)/shard_map/psum | solution.py:52
  203.8 9.4 %all-reduce.3 = (f32[]{:T(128)}, f32[]{:T(128)}) all-reduce(f32[]{:T(128)} %get-tuple-element.8, f32[]{:T(128)} %get-tuple-element.9), channel_id=1, replica_groups=mesh['fs_0'=4,'fs_1'=4,'rep'=4,'tp'=2] {'tp'}, use_global_device_ids=true, to_apply=%region_5.0 | all-reduce | flops 2 | bytes 16 | tf_op jit(solution)/shard_map/psum | solution.py:52
  214.5 27.6 %all-gather.6.cloned.1.call-done = bf16[512,2560]{1,0:T(8,128)(2,1)} async-done(((bf16[8,2560]{1,0:T(8,128)(2,1)}), bf16[512,2560]{1,0:T(8,128)(2,1)}) %all-gather.6.cloned.1.call-update) | async-done | bytes 2621456 | tf_op jit(solution)/shard_map/all_gather | solution.py:58
  243.5 2.1 fusion.1
  246.4 46.2 %all-gather.10.cloned.1.call-done = bf16[1572864]{0:T(1024)(128)(2,1)} async-done(((bf16[98304]{0:T(1024)(128)(2,1)}), bf16[1572864]{0:T(1024)(128)(2,1)}) %all-gather.10.cloned.1.call-update) | async-done | bytes 3145744 | tf_op jit(solution)/shard_map/all_gather | solution.py:30
  292.6 3.9 %reshape.41 = bf16[16,98304]{1,0:T(8,128)(2,1)} reshape(bf16[1572864]{0:T(1024)(128)(2,1)} %all-gather.10.cloned.1.call-done) | data formatting | bytes 6291456 | tf_op jit(solution)/shard_map/all_gather | solution.py:30
  296.5 2.3 slice.28
  298.8 1.6 slice-done.1
  300.4 1.9 reshape_reshape.15
  302.3 2.3 reshape_reshape.14
  (64 shorter events, 10.1 us)
Async XLA Ops:
  7.2 110.5 %copy-start = (bf16[1024,512]{1,0:T(8,128)(2,1)S(1)}, bf16[1024,512]{1,0:T(8,128)(2,1)}, u32[]{:S(2)}) copy-start(bf16[1024,512]{1,0:T(8,128)(2,1)} %param.13) | copy-start | bytes 3145732
  7.2 78.9 %all-gather.8.cloned.1.call-start = ((), (), s32[]{:S(2)}) async-start(), calls=%async_computation.3 | async-start | bytes 6389760 | tf_op jit(solution)/shard_map/all_gather | solution.py:30
  99.5 7.6 %slice-start = ((bf16[64,49152]{1,0:T(8,128)(2,1)}), bf16[64,16384]{1,0:T(8,128)(2,1)S(1)}, s32[]{:S(2)}) async-start(bf16[64,49152]{1,0:T(8,128)(2,1)} %reshape.40), calls=%async_computation.5 | async-start | bytes 4194304 | tf_op jit(solution)/shard_map/slice | solution.py:32
  118.3 9.9 %copy-start.2 = (bf16[2048,512]{1,0:T(8,128)(2,1)S(1)}, bf16[2048,512]{1,0:T(8,128)(2,1)}, u32[]{:S(2)}) copy-start(bf16[2048,512]{1,0:T(8,128)(2,1)} %reshape_reshape.13) | copy-start | bytes 6291460
  119.9 19.9 %all-to-all-start = ((bf16[64,8,512]{2,1,0:T(8,128)(2,1)}), bf16[64,8,512]{2,1,0:T(8,128)(2,1)S(1)}, u32[]{:S(2)}, u32[]{:S(2)}) async-start(bf16[64,8,512]{2,1,0:T(8,128)(2,1)} %fusion.6), calls=%async_computation | async-start | bytes 1048576 | tf_op jit(solution)/shard_map/all_to_all | solution.py:46
  128.2 4.7 %copy-start.17 = (bf16[1024,2048]{1,0:T(8,128)(2,1)S(1)}, bf16[1024,2048]{1,0:T(8,128)(2,1)}, u32[]{:S(2)}) copy-start(bf16[1024,2048]{1,0:T(8,128)(2,1)} %param.15) | copy-start | bytes 12582916
  139.0 10.3 %copy-start.15 = (f32[8,512]{1,0:T(8,128)S(1)}, f32[8,512]{1,0:T(8,128)}, u32[]{:S(2)}) copy-start(f32[8,512]{1,0:T(8,128)} %param.21) | copy-start | bytes 49156
  139.0 10.3 %copy-start.16 = (f32[8,512]{1,0:T(8,128)S(1)}, f32[8,512]{1,0:T(8,128)}, u32[]{:S(2)}) copy-start(f32[8,512]{1,0:T(8,128)} %param.20) | copy-start | bytes 49156
  139.0 37.4 %copy-start.11 = (f32[8,2048]{1,0:T(8,128)S(1)}, f32[8,2048]{1,0:T(8,128)}, u32[]{:S(2)}) copy-start(f32[8,2048]{1,0:T(8,128)} %param.23) | copy-start | bytes 196612
  139.0 37.4 %copy-start.12 = (f32[8,2048]{1,0:T(8,128)S(1)}, f32[8,2048]{1,0:T(8,128)}, u32[]{:S(2)}) copy-start(f32[8,2048]{1,0:T(8,128)} %param.22) | copy-start | bytes 196612
  139.8 36.3 %all-to-all-start.1 = ((bf16[64,8,2048]{2,1,0:T(8,128)(2,1)}), bf16[64,8,2048]{2,1,0:T(8,128)(2,1)S(1)}, u32[]{:S(2)}, u32[]{:S(2)}) async-start(bf16[64,8,2048]{2,1,0:T(8,128)(2,1)} %fusion), calls=%async_computation.1 | async-start | bytes 4194304 | tf_op jit(solution)/shard_map/all_to_all | solution.py:46
  149.1 93.0 %copy-start.5 = (bf16[64,512]{1,0:T(8,128)(2,1)S(1)}, bf16[64,512]{1,0:T(8,128)(2,1)}, u32[]{:S(2)}) copy-start(bf16[64,512]{1,0:T(8,128)(2,1)} %param.18) | copy-start | bytes 196612
  149.1 94.2 %copy-start.9 = (f32[64,512]{1,0:T(8,128)S(1)}, f32[64,512]{1,0:T(8,128)}, u32[]{:S(2)}) copy-start(f32[64,512]{1,0:T(8,128)} %param.16) | copy-start | bytes 393220
  149.1 94.3 %copy-start.10 = (bf16[32,512]{1,0:T(8,128)(2,1)S(1)}, bf16[32,512]{1,0:T(8,128)(2,1)}, u32[]{:S(2)}) copy-start(bf16[32,512]{1,0:T(8,128)(2,1)} %param.19) | copy-start | bytes 98308
  149.1 93.0 %all-gather.6.cloned.1.call-start = ((), (), s32[]{:S(2)}) async-start(), calls=%async_computation.2 | async-start | bytes 2662400 | tf_op jit(solution)/shard_map/all_gather | solution.py:58
  149.9 93.5 %copy-start.14 = (f32[8,512]{1,0:T(8,128)}, f32[8,512]{1,0:T(8,128)S(1)}, u32[]{:S(2)}) copy-start(f32[8,512]{1,0:T(8,128)S(1)} %get-tuple-element.21) | copy-start | bytes 49156
  149.9 95.6 %copy-start.13 = (f32[8,512]{1,0:T(8,128)}, f32[8,512]{1,0:T(8,128)S(1)}, u32[]{:S(2)}) copy-start(f32[8,512]{1,0:T(8,128)S(1)} %get-tuple-element.20) | copy-start | bytes 49156
  176.4 69.1 %copy-start.8 = (f32[32,2048]{1,0:T(8,128)S(1)}, f32[32,2048]{1,0:T(8,128)}, u32[]{:S(2)}) copy-start(f32[32,2048]{1,0:T(8,128)} %param.17) | copy-start | bytes 786436
  177.1 66.4 %copy-start.7 = (f32[8,2048]{1,0:T(8,128)}, f32[8,2048]{1,0:T(8,128)S(1)}, u32[]{:S(2)}) copy-start(f32[8,2048]{1,0:T(8,128)S(1)} %get-tuple-element.18) | copy-start | bytes 196612
  177.1 68.5 %copy-start.6 = (f32[8,2048]{1,0:T(8,128)}, f32[8,2048]{1,0:T(8,128)S(1)}, u32[]{:S(2)}) copy-start(f32[8,2048]{1,0:T(8,128)S(1)} %get-tuple-element.17) | copy-start | bytes 196612
  177.7 114.8 %all-gather.10.cloned.1.call-start = ((), (), s32[]{:S(2)}) async-start(), calls=%async_computation.4 | async-start | bytes 3342336 | tf_op jit(solution)/shard_map/all_gather | solution.py:30
  243.4 53.1 %copy-start.4 = (f32[64,512]{1,0:T(8,128)}, f32[64,512]{1,0:T(8,128)S(1)}, u32[]{:S(2)}) copy-start(f32[64,512]{1,0:T(8,128)S(1)} %fusion.7) | copy-start | bytes 393220
  245.6 50.9 %copy-start.3 = (f32[32,2048]{1,0:T(8,128)}, f32[32,2048]{1,0:T(8,128)S(1)}, u32[]{:S(2)}) copy-start(f32[32,2048]{1,0:T(8,128)S(1)} %fusion.1) | copy-start | bytes 786436
  298.8 5.9 %copy-start.1 = (bf16[1024,512]{1,0:T(8,128)(2,1)S(1)}, bf16[1024,512]{1,0:T(8,128)(2,1)}, u32[]{:S(2)}) copy-start(bf16[1024,512]{1,0:T(8,128)(2,1)} %param.13) | copy-start | bytes 3145732
  (1 other events, 1.6 us)
Sparse Core Ops, SparseCore 0:
  11.4 74.6 all-gather.7
  177.9 64.1 all-gather.5
  246.5 46.0 all-gather.9
where the time goes:
time: 312 us; the launch traced here: 311 us
  waiting for transfers between devices  177 us (57%)
  local copies, waits for them, and re-layouts  37.2 us (12%)
  blocking collectives  35.3 us (11%)
  matrix products  24.5 us (8%)
  starting transfers between devices  17.8 us (6%)
  between operations  15.4 us (5%)
  other arithmetic  3.72 us (1%)
    all_gather x2, waiting for transfers between devices, gather_together(): lines, at, gathered = (lax.all_gather(ravelled, axis), 0, [])  123 us
    psum x4, blocking collectives, over_axes(): value = lax.psum(value, axis)  35.3 us
    all_gather x1, waiting for transfers between devices, sent_together(): lax.all_gather(both, axis, axis=dim, tiled=True)  27.6 us
    all_to_all x2, waiting for transfers between devices, summed_on_arrival(): tiles = lax.all_to_all(in_blocks(value, dim, count), axis, 0, 0, tiled=True)  27 us
    all_to_all x2, starting transfers between devices, summed_on_arrival(): tiles = lax.all_to_all(in_blocks(value, dim, count), axis, 0, 0, tiled=True)  17.6 us
    another operation x4, local copies, waits for them, and re-layouts, joined_along(): tiles.reshape(*shape[:dim], shape[dim] * shape[dim + 1], *shape[dim + 2:])  14.2 us
    all_gather x2, local copies, waits for them, and re-layouts, gather_together(): lines, at, gathered = (lax.all_gather(ravelled, axis), 0, [])  12.8 us
    slice x6, local copies, waits for them, and re-layouts, gather_together(): tiles = lines[:, at:at + a.size].reshape(-1, *a.shape)  8.41 us
  transfers between devices with their start and end apart: 5, of which 5 were waited for; matrix products, arithmetic and copies ran while one was open for 4% of the time, Pallas kernels for 0%

commit v1 on v0

v1 whole, which is shorter than its diff:
```python
import functools

import jax
import jax.numpy as jnp
from jax import lax
from jax.experimental import pallas as pl
from jax.experimental.pallas import tpu as pltpu
from jax.sharding import Mesh
from jax.sharding import PartitionSpec as P

D = 4096
QKW = 1024
VW = 2048
R = 512
FS = ("fs_0", "fs_1")
REP_FS = ("rep", "fs_0", "fs_1")
FS_REP = ("fs_0", "fs_1", "rep")
AXES = ("rep", "fs_0", "fs_1")
ORDERS = (("fs_1", "fs_0", "rep"), ("fs_0", "rep", "fs_1"), ("rep", "fs_1", "fs_0"))

beta_first = 0.6
beta_second = 0.8
step_rate = 0.01
small_eps = 1e-06

MESH = pl.DeviceIdType.MESH
ANY = pl.BlockSpec(memory_space=pl.ANY)
VMEM = pl.BlockSpec(memory_space=pltpu.VMEM)
BF = jnp.bfloat16
F32 = jnp.float32
WIDE = 2688


def moments(first, second, projected):
    first_next = beta_first * first + (1.0 - beta_first) * projected
    second_next = beta_second * second + (1.0 - beta_second) * projected * projected
    return (first_next, second_next, first_next * lax.rsqrt(second_next))


def block_at(order, k, slot, coord):
    out = []
    for axis in AXES:
        if axis in order[:k]:
            out.append(slice(None))
        elif axis == order[k]:
            out.append(slot)
        else:
            out.append(coord[axis])
    return tuple(out)


def step_of(coord, axis, d):
    return lax.rem(coord[axis] + d, 4)


def sending(src, dst, ss, rs, at, axis, to):
    return pltpu.make_async_remote_copy(
        src_ref=src,
        dst_ref=dst,
        send_sem=ss.at[at],
        recv_sem=rs.at[at],
        device_id={axis: to},
        device_id_type=MESH,
    )


class Gather:
    def __init__(self, buf, order, k, low, high, coord, ss, rs, base):
        axis = order[k]
        right, left = step_of(coord, axis, 1), step_of(coord, axis, 3)

        def at(slot, half):
            return buf.at[block_at(order, k, slot, coord) + half]

        me = coord[axis]
        mk = lambda ref, n, to: sending(ref, ref, ss, rs, base + n, axis, to)
        self.first = [
            mk(at(me, low), 0, right),
            mk(at(me, high), 1, left),
            mk(at(me, high), 2, right),
            mk(at(me, low), 3, left),
        ]
        self.forward = [mk(at(left, low), 4, right), mk(at(right, high), 5, left)]

    def start(self):
        for c in self.first:
            c.start()

    def pass_on(self):
        for n in range(2):
            self.first[n].wait_recv()
            self.forward[n].start()

    def arrive(self):
        self.first[2].wait_recv()
        self.first[3].wait_recv()
        self.forward[0].wait_recv()
        self.forward[1].wait_recv()

    def sent(self):
        for c in self.first + self.forward:
            c.wait_send()


class Reduce:
    def __init__(self, buf, order, k, low, high, coord, ss, rs, base, from_left, from_right, mid_low, mid_high):
        axis = order[k]
        me = coord[axis]
        right, left, far = (step_of(coord, axis, d) for d in (1, 3, 2))
        self.at = lambda slot, half: block_at(order, k, slot, coord) + half
        self.buf, self.low, self.high = buf, low, high
        self.me, self.right, self.left = me, right, left
        self.from_left, self.from_right = from_left, from_right
        self.mid_low, self.mid_high = mid_low, mid_high
        n = len(block_at(order, k, me, coord))
        lead = sum(isinstance(i, slice) for i in block_at(order, k, me, coord))
        whole = (slice(None),) * lead
        start = low[-1].start

        def part(ref, half):
            h = half[-1]
            return ref.at[whole + (slice(None), slice(h.start - start, h.stop - start))]

        src = lambda slot, half: buf.at[self.at(slot, half)]
        mk = lambda s, d, i, to: sending(s, d, ss, rs, base + i, axis, to)
        self.first = [
            mk(src(far, low), mid_low, 0, right),
            mk(src(far, high), mid_high, 1, left),
            mk(src(right, high), part(from_left, high), 2, right),
            mk(src(left, low), part(from_right, low), 3, left),
        ]
        self.second = [
            mk(src(right, low), part(from_left, low), 4, right),
            mk(src(left, high), part(from_right, high), 5, left),
        ]

    def start(self):
        for c in self.first:
            c.start()

    def pass_on(self):
        self.first[0].wait_recv()
        i = self.at(self.right, self.low)
        self.buf[i] = (self.buf[i].astype(F32) + self.mid_low[...].astype(F32)).astype(BF)
        self.second[0].start()
        self.first[1].wait_recv()
        i = self.at(self.left, self.high)
        self.buf[i] = (self.buf[i].astype(F32) + self.mid_high[...].astype(F32)).astype(BF)
        self.second[1].start()

    def total(self):
        self.first[2].wait_recv()
        self.first[3].wait_recv()
        self.second[0].wait_recv()
        self.second[1].wait_recv()
        i = self.at(self.me, (slice(None), slice(self.low[-1].start, self.high[-1].stop)))
        own = self.buf[i].astype(F32)
        return i, own + self.from_left[...].astype(F32) + self.from_right[...].astype(F32)

    def sent(self):
        for c in self.first + self.second:
            c.wait_send()


def kernel(*refs):
    (x_hbm, cq_hbm, br_hbm, co_hbm, bq_hbm, bo_hbm, fq, sq, fo, so) = refs[:10]
    (fqn, sqn, fon, son, normed_out, sums_out) = refs[10:16]
    (x, br, cq, co, bq, bo, tq, to, p, n, proj, sums, psums) = refs[16:29]
    scratch = refs[29:29 + 36]
    (lsem, ags, agr, rss, rsr, ngs, ngr, psem_s, psem_r) = refs[65:]

    coord = {a: lax.axis_index(a) for a in AXES}
    core = lax.axis_index("tp")
    partner = 1 - core
    own = (coord["rep"], coord["fs_0"], coord["fs_1"])

    half = pl.ds(pl.multiple_of(core * 256, 256), 256)
    own_q = pltpu.make_async_copy(bq_hbm.at[:, half], bq.at[own], lsem.at[0])
    own_o = pltpu.make_async_copy(bo_hbm.at[:, half], bo.at[own], lsem.at[1])
    loads = [
        pltpu.make_async_copy(x_hbm, x, lsem.at[2]),
        pltpu.make_async_copy(br_hbm, br, lsem.at[3]),
        pltpu.make_async_copy(cq_hbm, cq, lsem.at[4]),
        pltpu.make_async_copy(co_hbm, co, lsem.at[5]),
    ]
    own_q.start()
    own_o.start()

    barrier = pltpu.get_barrier_semaphore()
    for axis in AXES:
        for d in (1, 3):
            pl.semaphore_signal(barrier, inc=1, device_id={axis: step_of(coord, axis, d)}, device_id_type=MESH)
    pl.semaphore_signal(barrier, inc=1, device_id={"tp": partner}, device_id_type=MESH)
    own_q.wait()
    own_o.wait()
    for c in loads:
        c.start()
    pl.semaphore_wait(barrier, 7)

    everything = slice(None)
    parts = ((bq, 0), (bq, 32), (bo, 0))
    done = []
    for k in range(3):
        phase = []
        for i, (buf, row) in enumerate(parts):
            low = (slice(row, row + 16), everything)
            high = (slice(row + 16, row + 32), everything)
            phase.append(Gather(buf, ORDERS[i], k, low, high, coord, ags, agr, (k * 3 + i) * 6))
        for g in phase:
            g.start()
        for g in phase:
            g.pass_on()
        for g in phase:
            g.arrive()
        done += phase

    for c in loads:
        c.wait()

    tiles = 256

    @pl.loop(0, 1024 // tiles)
    def _(t):
        rows = pl.ds(pl.multiple_of(t * tiles, tiles), tiles)
        acc = jnp.dot(x[rows, :], bq[...].reshape(4096, 256), preferred_element_type=F32)
        tq[core, :, rows] = acc.T.astype(BF)

    def to_partner(ref, i):
        return pltpu.make_async_remote_copy(
            src_ref=ref.at[core], dst_ref=ref.at[core], send_sem=psem_s.at[i], recv_sem=psem_r.at[i],
            device_id={"tp": partner}, device_id_type=MESH)

    swap_q = to_partner(tq, 0)
    swap_q.start()

    @pl.loop(0, 1024 // tiles)
    def _(t):
        rows = pl.ds(pl.multiple_of(t * tiles, tiles), tiles)
        acc = jnp.dot(br[rows, :], bo[...].reshape(2048, 256), preferred_element_type=F32)
        to[core, :, rows] = acc.T.astype(BF)

    swap_o = to_partner(to, 1)
    swap_o.start()

    def project(h):
        blocks = pl.ds(2 * h, 2)
        acc = jnp.dot(tq[h], cq[...], preferred_element_type=F32)
        p[blocks, :, :, :, 0:512] = acc.reshape(2, 4, 4, 8, 512).astype(BF)

        @pl.loop(0, 4)
        def _(t):
            cols = pl.ds(pl.multiple_of(t * 512, 512), 512)
            dest = pl.ds(pl.multiple_of(512 + t * 512, 512), 512)
            acc = jnp.dot(to[h], co[:, cols], preferred_element_type=F32)
            p[blocks, :, :, :, dest] = acc.reshape(2, 4, 4, 8, 512).astype(BF)

    project(core)
    swap_q.wait_recv()
    swap_o.wait_recv()
    project(partner)

    halves = (
        ((everything, slice(0, 512)), (everything, slice(512, 896))),
        ((everything, slice(896, 1408)), (everything, slice(1408, 1792))),
        ((everything, slice(1792, 2176)), (everything, slice(2176, 2560))),
    )
    for j, k in enumerate((2, 1, 0)):
        phase = []
        for i, (low, high) in enumerate(halves):
            bufs = scratch[(j * 3 + i) * 4:(j * 3 + i) * 4 + 4]
            phase.append(Reduce(p, ORDERS[i], k, low, high, coord, rss, rsr, (j * 3 + i) * 6, *bufs))
        for g in phase:
            g.start()
        for g in phase:
            g.pass_on()
        for i, g in enumerate(phase):
            at, total = g.total()
            if k:
                p[at] = total.astype(BF)
            else:
                proj[:, at[-1]] = total
        done += phase

    first_q, second_q, normed_q = moments(fq[...], sq[...], proj[:, 0:512])
    first_o, second_o, normed_o = moments(fo[...], so[...], proj[:, 512:2560])
    n[own + (everything, slice(0, 512))] = normed_q.astype(BF)
    n[own + (everything, slice(512, 2560))] = normed_o.astype(BF)
    lane = lax.broadcasted_iota(jnp.int32, (8, 128), 1)
    tile = jnp.zeros((8, 128), F32)
    for base, normed in ((0, normed_q), (3, normed_o)):
        rest = jnp.broadcast_to(jnp.sum(normed * normed, keepdims=True), (8, 128))
        for e in range(3):
            top = rest.astype(BF).astype(F32)
            tile = jnp.where(lane == base + e, top, tile)
            rest = rest - top
    n[own + (everything, slice(2560, 2688))] = tile.astype(BF)
    fqn[...] = first_q
    sqn[...] = second_q
    fon[...] = first_o
    son[...] = second_o

    halves = (
        ((everything, slice(0, 512)), (everything, slice(512, 896))),
        ((everything, slice(896, 1408)), (everything, slice(1408, 1792))),
        ((everything, slice(1792, 2304)), (everything, slice(2304, 2688))),
    )
    for k in range(3):
        phase = []
        for i, (low, high) in enumerate(halves):
            phase.append(Gather(n, ORDERS[i], k, low, high, coord, ngs, ngr, (k * 3 + i) * 6))
        for g in phase:
            g.start()
        for g in phase:
            g.pass_on()
        for g in phase:
            g.arrive()
        done += phase

    out = pltpu.make_async_copy(n, normed_out, lsem.at[6])
    out.start()
    sums[...] = jnp.sum(n[:, :, :, :, 2560:2688].astype(F32), axis=(0, 1, 2))
    swap_s = pltpu.make_async_remote_copy(
        src_ref=sums, dst_ref=psums, send_sem=psem_s.at[2], recv_sem=psem_r.at[2],
        device_id={"tp": partner}, device_id_type=MESH)
    swap_s.start()
    swap_s.wait_recv()
    both = sums[...] + psums[...]
    total_q = jnp.sum(jnp.where(lane < 3, both, 0.0), axis=1, keepdims=True)
    total_o = jnp.sum(jnp.where((lane >= 3) & (lane < 6), both, 0.0), axis=1, keepdims=True)
    scale_q = lax.rsqrt(total_q / (R * QKW) + small_eps)
    scale_o = lax.rsqrt(total_o / (R * D) + small_eps)
    sums_out[...] = jnp.where(lane == 0, scale_q, scale_o)
    for c in done:
        c.sent()
    for c in (swap_q, swap_o, swap_s):
        c.wait_send()
    out.wait()


def scratch_for_reduce():
    shapes = []
    widths = ((512, 384), (512, 384), (384, 384))
    for j, lead in enumerate(((4, 4), (4,), ())):
        for low, high in widths:
            shapes += [
                pltpu.VMEM(lead + (8, low + high), BF),
                pltpu.VMEM(lead + (8, low + high), BF),
                pltpu.VMEM(lead + (8, low), BF),
                pltpu.VMEM(lead + (8, high), BF),
            ]
    return shapes


def gathered_moments(x, cq, br, co, bq, bo, fq, sq, fo, so):
    sds = jax.ShapeDtypeStruct
    dma = pltpu.SemaphoreType.DMA
    return pl.pallas_call(
        kernel,
        out_shape=(
            sds((8, 512), F32), sds((8, 512), F32), sds((8, 2048), F32), sds((8, 2048), F32),
            sds((4, 4, 4, 8, WIDE), BF), sds((8, 128), F32),
        ),
        in_specs=[ANY] * 6 + [VMEM] * 4,
        out_specs=(VMEM, VMEM, VMEM, VMEM, ANY, VMEM),
        scratch_shapes=[
            pltpu.VMEM((1024, 4096), BF), pltpu.VMEM((1024, 2048), BF),
            pltpu.VMEM((1024, 512), BF), pltpu.VMEM((1024, 2048), BF),
            pltpu.VMEM((4, 4, 4, 64, 256), BF), pltpu.VMEM((4, 4, 4, 32, 256), BF),
            pltpu.VMEM((2, 256, 1024), BF), pltpu.VMEM((2, 256, 1024), BF),
            pltpu.VMEM((4, 4, 4, 8, WIDE), BF), pltpu.VMEM((4, 4, 4, 8, WIDE), BF),
            pltpu.VMEM((8, 2560), F32), pltpu.VMEM((8, 128), F32), pltpu.VMEM((8, 128), F32),
            *scratch_for_reduce(),
            dma((7,)), dma((54,)), dma((54,)), dma((54,)), dma((54,)), dma((54,)), dma((54,)),
            dma((3,)), dma((3,)),
        ],
        compiler_params=pltpu.CompilerParams(
            collective_id=0, has_side_effects=True, vmem_limit_bytes=60 * 1024 * 1024),
        name="moments_everywhere",
    )(x, cq, br, co, bq, bo, fq, sq, fo, so)


def gather_together(arrays, axis):
    ravelled = jnp.concatenate([a.reshape(-1) for a in arrays])
    lines, at, gathered = (lax.all_gather(ravelled, axis), 0, [])
    for a in arrays:
        tiles = lines[:, at : at + a.size].reshape(-1, a.shape[1])
        gathered.append(tiles)
        at += a.size
    return tuple(gathered)


def body(query_input, query_cotangent, branch_output, layer_cotangent, query_weight, output_weight,
         query_basis, output_basis, query_first, query_second, output_first, output_second):
    first_q, second_q, first_o, second_o, normed, scales = gathered_moments(
        query_input, query_cotangent, branch_output, layer_cotangent, query_basis, output_basis,
        query_first, query_second, output_first, output_second)
    rows = normed.reshape(R, WIDE)
    update_q = scales[0, 0] * jnp.dot(query_basis, rows[:, 0:512], preferred_element_type=F32)
    update_o = scales[0, 1] * jnp.dot(output_basis, rows[:, 512:2560], preferred_element_type=F32)
    query_copy, output_copy = gather_together(
        ((query_weight - step_rate * update_q).astype(BF), (output_weight - step_rate * update_o).astype(BF)), FS)
    return (update_q, update_o, first_q, second_q, first_o, second_o, query_copy, output_copy)


def solution(mesh):
    split = Mesh(
        mesh.devices.reshape(4, 4, mesh.shape["rep"], mesh.shape["tp"]),
        ("fs_0", "fs_1", "rep", "tp"),
    )
    tokens, rows = P(FS_REP, None), P(REP_FS, "tp")
    return jax.shard_map(
        body,
        mesh=split,
        in_specs=(tokens, P(FS_REP, "tp"), tokens, P(FS_REP, "tp"), rows, rows,
                  P(REP_FS, None), P(REP_FS, None), rows, rows, rows, rows),
        out_specs=(rows, rows, rows, rows, rows, rows, P("rep", "tp"), P("rep", "tp")),
        check_vma=False,
    )
```

time: 312 us -> 172 us (0.55)
  waiting for transfers between devices: 177 us -> 44.1 us
  Pallas kernels: 0 us -> 94.7 us
  blocking collectives: 35.3 us -> 0 us
  local copies, waits for them, and re-layouts: 37.2 us -> 13.7 us
  matrix products: 24.5 us -> 4.64 us
  starting transfers between devices: 17.8 us -> 0.04 us
    pallas_call x0 -> x1, Pallas kernels: none -> 94.7 us  [gathered_moments(): pl.pallas_call(kernel, out_shape=(sds((8, 512), F32), sds((8, 512), F32),...]
    all_gather x2 -> x1, waiting for transfers between devices: 123 us -> 44.1 us  [gather_together(): lines, at, gathered = (lax.all_gather(ravelled, axis), 0, [])]
    psum x4 -> x0, blocking collectives: 35.3 us -> none  [over_axes(): value = lax.psum(value, axis)]
    all_gather x1 -> x0, waiting for transfers between devices: 27.6 us -> none  [sent_together(): lax.all_gather(both, axis, axis=dim, tiled=True)]
    all_to_all x2 -> x0, waiting for transfers between devices: 27 us -> none  [summed_on_arrival(): tiles = lax.all_to_all(in_blocks(value, dim, count), axis, 0, 0, tiled=True)]
    dot_general x8 -> x2, matrix products: 24.5 us -> 4.64 us  [the longest x1 2.75 us: body(): jnp.dot(output_basis, rows[:, 512:2560], preferred_element_type=F32)]
    all_to_all x2 -> x0, starting transfers between devices: 17.6 us -> none  [summed_on_arrival(): tiles = lax.all_to_all(in_blocks(value, dim, count), axis, 0, 0, tiled=True)]
    another operation x4 -> x0, local copies, waits for them, and re-layouts: 14.2 us -> none  [joined_along(): tiles.reshape(*shape[:dim], shape[dim] * shape[dim + 1], *shape[dim + 2:])]
  transfers between devices with their start and end apart: 5 -> 1, of which waited for: 5 -> 1; matrix products, arithmetic and copies ran while one was open for 4% -> 0% of each run, Pallas kernels for 0% -> 0%
where the time goes in v1:
time: 172 us
  Pallas kernels  94.7 us (55%)
  waiting for transfers between devices  44.1 us (26%)
  between operations  14.2 us (8%)
  local copies, waits for them, and re-layouts  13.7 us (8%)
  matrix products  4.64 us (3%)
    pallas_call x1, Pallas kernels, gathered_moments(): pl.pallas_call(kernel, out_shape=(sds((8, 512), F32), sds((8, 512), F32),...  94.7 us
    all_gather x1, waiting for transfers between devices, gather_together(): lines, at, gathered = (lax.all_gather(ravelled, axis), 0, [])  44.1 us
    reshape x2, local copies, waits for them, and re-layouts, gather_together(): tiles = lines[:, at:at + a.size].reshape(-1, a.shape[1])  4.54 us
  transfers between devices with their start and end apart: 1, of which 1 were waited for; matrix products, arithmetic and copies ran while one was open for 0% of the time, Pallas kernels for 0%

profile of v1, /device:TPU:1, one launch (start us, length us, event | category | flops | bytes accessed | tf_op | source)
XLA Modules:
  0.0 172.1 jit_solution(9648242748121957823)
XLA Ops:
  7.2 0.0 copy-start.5
  7.2 0.0 copy-start.3
  7.2 0.0 all-gather.3.cloned.1.call-start
  7.2 94.7 %moments_everywhere.1 = (f32[8,512]{1,0:T(8,128)}, f32[8,512]{1,0:T(8,128)}, f32[8,2048]{1,0:T(8,128)}, f32[8,2048]{1,0:T(8,128)}, bf16[4,4,4,8,2688]{4,3,2,1,0:T(8,128)(2,1)}, /*index=5*/f32[8,128]{1,0:T(8,128)}) custom-call(bf16[1024,4096]{1,0:T(8,128)(2,1)} %refs_0_.1, bf16[1024,512]{1,0:T(8,128)(2,1)} %refs_1_.1, bf16[1024,2048]{1,0:T(8,128)(2,1)} %refs_2_.1, ...), custom_call_target="tpu_custom_call" | custom-call | tf_op jit(solution)/shard_map/moments_everywhere/pallas_call | solution.py:357
  101.9 0.0 copy-start.6
  101.9 0.0 copy-start.4
  102.0 1.3 fusion.6
  103.3 1.9 %fusion.2 = f32[64,512]{1,0:T(8,128)S(1)} fusion(bf16[64,512]{1,0:T(8,128)(2,1)S(1)} %copy-done.3, bf16[512,2688]{1,0:T(8,128)(2,1)} %bitcast.15, f32[]{:T(128)} %bitcast), kind=kOutput, calls=%fused_computation.4 | convolution fusion | flops 33587200 | bytes 721408 | tf_op jit(solution)/shard_map/dot_general | solution.py:398
  105.2 0.0 copy-start.2
  105.2 2.7 %fusion = f32[32,2048]{1,0:T(8,128)S(1)} fusion(bf16[32,512]{1,0:T(8,128)(2,1)S(1)} %copy-done.5, bf16[512,2688]{1,0:T(8,128)(2,1)} %bitcast.16, f32[]{:T(128)} %bitcast.3), kind=kOutput, calls=%fused_computation.1 | convolution fusion | flops 67174400 | bytes 2392576 | tf_op jit(solution)/shard_map/dot_general | solution.py:399
  108.0 0.0 copy-done.6
  108.0 0.0 copy-start.1
  108.1 0.7 pad_maximum_fusion
  108.8 0.0 all-gather.3.cloned.1.call-update
  108.9 44.1 %all-gather.3.cloned.1.call-done = bf16[1572864]{0:T(1024)(128)(2,1)} async-done(((bf16[98304]{0:T(1024)(128)(2,1)}), bf16[1572864]{0:T(1024)(128)(2,1)}) %all-gather.3.cloned.1.call-update) | async-done | bytes 3145744 | tf_op jit(solution)/shard_map/all_gather | solution.py:384
  152.9 2.8 %reshape.36 = bf16[16,98304]{1,0:T(8,128)(2,1)S(1)} reshape(bf16[1572864]{0:T(1024)(128)(2,1)} %all-gather.3.cloned.1.call-done) | data formatting | bytes 6291456 | tf_op jit(solution)/shard_map/all_gather | solution.py:384
  155.7 1.0 slice.26
  156.8 1.5 slice.27
  158.3 3.3 %reshape.35 = bf16[512,2048]{1,0:T(8,128)(2,1)} reshape(bf16[16,65536]{1,0:T(8,128)(2,1)} %slice.27) | data formatting | bytes 4194304 | tf_op jit(solution)/shard_map/reshape | solution.py:386
  161.5 1.3 reshape.34
  162.8 0.6 copy.26
  163.4 0.6 copy.27
  164.0 0.6 copy.28
  164.7 0.6 copy.29
  (19 shorter events, 0.1 us)
Async XLA Ops:
  7.2 98.0 %copy-start.5 = (bf16[32,512]{1,0:T(8,128)(2,1)S(1)}, bf16[32,512]{1,0:T(8,128)(2,1)}, u32[]{:S(2)}) copy-start(bf16[32,512]{1,0:T(8,128)(2,1)} %refs_5_.1) | copy-start | bytes 98308
  7.2 96.1 %copy-start.3 = (bf16[64,512]{1,0:T(8,128)(2,1)S(1)}, bf16[64,512]{1,0:T(8,128)(2,1)}, u32[]{:S(2)}) copy-start(bf16[64,512]{1,0:T(8,128)(2,1)} %refs_4_.1) | copy-start | bytes 196612
  7.2 145.8 %all-gather.3.cloned.1.call-start = ((), (), s32[]{:S(2)}) async-start(), calls=%async_computation | async-start | bytes 3342336 | tf_op jit(solution)/shard_map/all_gather | solution.py:384
  101.9 6.0 %copy-start.6 = (f32[64,512]{1,0:T(8,128)S(1)}, f32[64,512]{1,0:T(8,128)}, u32[]{:S(2)}) copy-start(f32[64,512]{1,0:T(8,128)} %param.16) | copy-start | bytes 393220
  101.9 6.1 %copy-start.4 = (f32[32,2048]{1,0:T(8,128)S(1)}, f32[32,2048]{1,0:T(8,128)}, u32[]{:S(2)}) copy-start(f32[32,2048]{1,0:T(8,128)} %param.17) | copy-start | bytes 786436
  105.2 50.5 %copy-start.2 = (f32[64,512]{1,0:T(8,128)}, f32[64,512]{1,0:T(8,128)S(1)}, u32[]{:S(2)}) copy-start(f32[64,512]{1,0:T(8,128)S(1)} %fusion.2) | copy-start | bytes 393220
  108.0 47.7 %copy-start.1 = (f32[32,2048]{1,0:T(8,128)}, f32[32,2048]{1,0:T(8,128)S(1)}, u32[]{:S(2)}) copy-start(f32[32,2048]{1,0:T(8,128)S(1)} %fusion) | copy-start | bytes 786436
  158.2 3.3 %copy-start = (bf16[16,32768]{1,0:T(8,128)(2,1)S(1)}, bf16[16,32768]{1,0:T(8,128)(2,1)}, u32[]{:S(2)}) copy-start(bf16[16,32768]{1,0:T(8,128)(2,1)} %slice.26) | copy-start | bytes 3145732
  158.2 4.6 %copy-start.10 = (f32[8,512]{1,0:T(8,128)S(1)}, f32[8,512]{1,0:T(8,128)}, u32[]{:S(2)}) copy-start(f32[8,512]{1,0:T(8,128)} %get-tuple-element.32) | copy-start | bytes 49156
  158.2 5.2 %copy-start.9 = (f32[8,512]{1,0:T(8,128)S(1)}, f32[8,512]{1,0:T(8,128)}, u32[]{:S(2)}) copy-start(f32[8,512]{1,0:T(8,128)} %get-tuple-element.33) | copy-start | bytes 49156
  158.2 5.8 %copy-start.8 = (f32[8,2048]{1,0:T(8,128)S(1)}, f32[8,2048]{1,0:T(8,128)}, u32[]{:S(2)}) copy-start(f32[8,2048]{1,0:T(8,128)} %get-tuple-element.34) | copy-start | bytes 196612
  158.3 6.4 %copy-start.7 = (f32[8,2048]{1,0:T(8,128)S(1)}, f32[8,2048]{1,0:T(8,128)}, u32[]{:S(2)}) copy-start(f32[8,2048]{1,0:T(8,128)} %get-tuple-element.35) | copy-start | bytes 196612
Sparse Core Ops, SparseCore 0:
  109.0 43.9 all-gather.2

commit v2 on v1

--- a/solution.py
+++ b/solution.py
@@ -39,7 +39,7 @@
 
 def block_at(order, k, slot, coord):
     out = []
-    for axis in AXES:
+    for axis in [a for a in AXES if a in order]:
         if axis in order[:k]:
             out.append(slice(None))
         elif axis == order[k]:
@@ -163,18 +163,20 @@
 
 
 def kernel(*refs):
-    (x_hbm, cq_hbm, br_hbm, co_hbm, bq_hbm, bo_hbm, fq, sq, fo, so) = refs[:10]
-    (fqn, sqn, fon, son, normed_out, sums_out) = refs[10:16]
-    (x, br, cq, co, bq, bo, tq, to, p, n, proj, sums, psums) = refs[16:29]
-    scratch = refs[29:29 + 36]
-    (lsem, ags, agr, rss, rsr, ngs, ngr, psem_s, psem_r) = refs[65:]
+    (x_hbm, cq_hbm, br_hbm, co_hbm, bq_hbm, bo_hbm, wq_in, wo_in, fq, sq, fo, so) = refs[:12]
+    (proj, scales_out, normed_out, bq_out, bo_out, wq_out, wo_out) = refs[12:19]
+    (x, br, cq, co, bq, bo, bq2, bo2, wq, wo, tq, to, p, n, sums, psums) = refs[19:35]
+    scratch = refs[35:71]
+    (lsem, ags, agr, rss, rsr, ngs, ngr, wgs, wgr, psem_s, psem_r) = refs[71:]
 
     coord = {a: lax.axis_index(a) for a in AXES}
     core = lax.axis_index("tp")
     partner = 1 - core
     own = (coord["rep"], coord["fs_0"], coord["fs_1"])
+    everything = slice(None)
 
     half = pl.ds(pl.multiple_of(core * 256, 256), 256)
+    other = pl.ds(pl.multiple_of(partner * 256, 256), 256)
     own_q = pltpu.make_async_copy(bq_hbm.at[:, half], bq.at[own], lsem.at[0])
     own_o = pltpu.make_async_copy(bo_hbm.at[:, half], bo.at[own], lsem.at[1])
     loads = [
@@ -196,23 +198,42 @@
     for c in loads:
         c.start()
     pl.semaphore_wait(barrier, 7)
-
-    everything = slice(None)
-    parts = ((bq, 0), (bq, 32), (bo, 0))
     done = []
-    for k in range(3):
+
+    def gathers(k, parts, ss, rs, orders=ORDERS):
         phase = []
-        for i, (buf, row) in enumerate(parts):
-            low = (slice(row, row + 16), everything)
-            high = (slice(row + 16, row + 32), everything)
-            phase.append(Gather(buf, ORDERS[i], k, low, high, coord, ags, agr, (k * 3 + i) * 6))
+        for i, (buf, low, high) in enumerate(parts):
+            phase.append(Gather(buf, orders[i], k, low, high, coord, ss, rs, (k * len(parts) + i) * 6))
         for g in phase:
             g.start()
+        done.extend(phase)
+        return phase
+
+    def pass_on(phase):
         for g in phase:
             g.pass_on()
+
+    def arrive(phase):
         for g in phase:
             g.arrive()
-        done += phase
+
+    def rows_of(buf, row):
+        return (buf, (slice(row, row + 16), everything), (slice(row + 16, row + 32), everything))
+
+    def cols_of(buf, a, b, c):
+        return (buf, (everything, slice(a, b)), (everything, slice(b, c)))
+
+    for k in range(3):
+        phase = gathers(k, (rows_of(bq, 0), rows_of(bq, 32), rows_of(bo, 0)), ags, agr)
+        if k == 0:
+            wq[own[1:]] = wq_in[...].astype(BF)
+            wo[own[1:]] = wo_in[...].astype(BF)
+        pass_on(phase)
+        arrive(phase)
+
+    weights = (cols_of(wo, 0, 768, 1536), cols_of(wo, 1536, 1792, 2048), cols_of(wq, 0, 256, 512))
+    turns = (("fs_0", "fs_1"), ("fs_1", "fs_0"), ("fs_1", "fs_0"))
+    carried = gathers(0, weights, wgs, wgr, turns)
 
     for c in loads:
         c.wait()
@@ -225,13 +246,14 @@
         acc = jnp.dot(x[rows, :], bq[...].reshape(4096, 256), preferred_element_type=F32)
         tq[core, :, rows] = acc.T.astype(BF)
 
-    def to_partner(ref, i):
+    def to_partner(src, dst, i):
         return pltpu.make_async_remote_copy(
-            src_ref=ref.at[core], dst_ref=ref.at[core], send_sem=psem_s.at[i], recv_sem=psem_r.at[i],
+            src_ref=src, dst_ref=dst, send_sem=psem_s.at[i], recv_sem=psem_r.at[i],
             device_id={"tp": partner}, device_id_type=MESH)
 
-    swap_q = to_partner(tq, 0)
+    swap_q = to_partner(tq.at[core], tq.at[core], 0)
     swap_q.start()
+    pass_on(carried)
 
     @pl.loop(0, 1024 // tiles)
     def _(t):
@@ -239,47 +261,60 @@
         acc = jnp.dot(br[rows, :], bo[...].reshape(2048, 256), preferred_element_type=F32)
         to[core, :, rows] = acc.T.astype(BF)
 
-    swap_o = to_partner(to, 1)
+    swap_o = to_partner(to.at[core], to.at[core], 1)
     swap_o.start()
-
-    def project(h):
-        blocks = pl.ds(2 * h, 2)
-        acc = jnp.dot(tq[h], cq[...], preferred_element_type=F32)
-        p[blocks, :, :, :, 0:512] = acc.reshape(2, 4, 4, 8, 512).astype(BF)
-
-        @pl.loop(0, 4)
-        def _(t):
-            cols = pl.ds(pl.multiple_of(t * 512, 512), 512)
-            dest = pl.ds(pl.multiple_of(512 + t * 512, 512), 512)
-            acc = jnp.dot(to[h], co[:, cols], preferred_element_type=F32)
-            p[blocks, :, :, :, dest] = acc.reshape(2, 4, 4, 8, 512).astype(BF)
-
-    project(core)
-    swap_q.wait_recv()
-    swap_o.wait_recv()
-    project(partner)
+    arrive(carried)
+    carried = gathers(1, weights, wgs, wgr, turns)
+    swap_bq = to_partner(bq.at[own[0]], bq2, 3)
+    swap_bo = to_partner(bo.at[own[0]], bo2, 4)
+    swap_bq.start()
+    swap_bo.start()
+
+    def project(h, t, c, a, b, at):
+        acc = jnp.dot(t[h], c[:, a:b], preferred_element_type=F32)
+        p[pl.ds(2 * h, 2), :, :, :, at:at + b - a] = acc.reshape(2, 4, 4, 8, b - a).astype(BF)
 
     halves = (
         ((everything, slice(0, 512)), (everything, slice(512, 896))),
         ((everything, slice(896, 1408)), (everything, slice(1408, 1792))),
         ((everything, slice(1792, 2176)), (everything, slice(2176, 2560))),
     )
-    for j, k in enumerate((2, 1, 0)):
-        phase = []
-        for i, (low, high) in enumerate(halves):
-            bufs = scratch[(j * 3 + i) * 4:(j * 3 + i) * 4 + 4]
-            phase.append(Reduce(p, ORDERS[i], k, low, high, coord, rss, rsr, (j * 3 + i) * 6, *bufs))
-        for g in phase:
-            g.start()
+
+    def reduces(j, i):
+        low, high = halves[i]
+        bufs = scratch[(j * 3 + i) * 4:(j * 3 + i) * 4 + 4]
+        g = Reduce(p, ORDERS[i], 2 - j, low, high, coord, rss, rsr, (j * 3 + i) * 6, *bufs)
+        g.start()
+        done.append(g)
+        return g
+
+    project(core, tq, cq, 0, 512, 0)
+    swap_q.wait_recv()
+    project(partner, tq, cq, 0, 512, 0)
+    project(core, to, co, 0, 384, 512)
+    swap_o.wait_recv()
+    project(partner, to, co, 0, 384, 512)
+    phase = [reduces(0, 0)]
+    for i, (a, b) in enumerate(((384, 1280), (1280, 2048))):
+        for h in range(2):
+            project(h, to, co, a, b, 512 + a)
+        phase.append(reduces(0, i + 1))
+    for g in phase:
+        g.pass_on()
+    for j in range(3):
+        later = []
+        for i, g in enumerate(phase):
+            at, total = g.total()
+            if j < 2:
+                p[at] = total.astype(BF)
+                later.append(reduces(j + 1, i))
+            else:
+                proj[:, at[-1]] = total
+        if j == 0:
+            pass_on(carried)
+        phase = later
         for g in phase:
             g.pass_on()
-        for i, g in enumerate(phase):
-            at, total = g.total()
-            if k:
-                p[at] = total.astype(BF)
-            else:
-                proj[:, at[-1]] = total
-        done += phase
 
     first_q, second_q, normed_q = moments(fq[...], sq[...], proj[:, 0:512])
     first_o, second_o, normed_o = moments(fo[...], so[...], proj[:, 512:2560])
@@ -294,34 +329,33 @@
             tile = jnp.where(lane == base + e, top, tile)
             rest = rest - top
     n[own + (everything, slice(2560, 2688))] = tile.astype(BF)
-    fqn[...] = first_q
-    sqn[...] = second_q
-    fon[...] = first_o
-    son[...] = second_o
-
-    halves = (
-        ((everything, slice(0, 512)), (everything, slice(512, 896))),
-        ((everything, slice(896, 1408)), (everything, slice(1408, 1792))),
-        ((everything, slice(1792, 2304)), (everything, slice(2304, 2688))),
-    )
+
+    swap_bq.wait_recv()
+    swap_bo.wait_recv()
+    outs = [
+        pltpu.make_async_copy(bq.at[own[0]], bq_out.at[:, :, :, half], lsem.at[7]),
+        pltpu.make_async_copy(bo.at[own[0]], bo_out.at[:, :, :, half], lsem.at[8]),
+        pltpu.make_async_copy(bq2, bq_out.at[:, :, :, other], lsem.at[9]),
+        pltpu.make_async_copy(bo2, bo_out.at[:, :, :, other], lsem.at[10]),
+    ]
+    late = [pltpu.make_async_copy(wq, wq_out, lsem.at[11]), pltpu.make_async_copy(wo, wo_out, lsem.at[12])]
+
     for k in range(3):
-        phase = []
-        for i, (low, high) in enumerate(halves):
-            phase.append(Gather(n, ORDERS[i], k, low, high, coord, ngs, ngr, (k * 3 + i) * 6))
-        for g in phase:
-            g.start()
-        for g in phase:
-            g.pass_on()
-        for g in phase:
-            g.arrive()
-        done += phase
+        phase = gathers(k, (cols_of(n, 0, 512, 896), cols_of(n, 896, 1408, 1792), cols_of(n, 1792, 2304, 2688)), ngs, ngr)
+        if k == 0:
+            for c in outs:
+                c.start()
+        pass_on(phase)
+        if k == 2:
+            arrive(carried)
+            for c in late:
+                c.start()
+        arrive(phase)
 
     out = pltpu.make_async_copy(n, normed_out, lsem.at[6])
     out.start()
     sums[...] = jnp.sum(n[:, :, :, :, 2560:2688].astype(F32), axis=(0, 1, 2))
-    swap_s = pltpu.make_async_remote_copy(
-        src_ref=sums, dst_ref=psums, send_sem=psem_s.at[2], recv_sem=psem_r.at[2],
-        device_id={"tp": partner}, device_id_type=MESH)
+    swap_s = to_partner(sums, psums, 2)
     swap_s.start()
     swap_s.wait_recv()
     both = sums[...] + psums[...]
@@ -329,12 +363,54 @@
     total_o = jnp.sum(jnp.where((lane >= 3) & (lane < 6), both, 0.0), axis=1, keepdims=True)
     scale_q = lax.rsqrt(total_q / (R * QKW) + small_eps)
     scale_o = lax.rsqrt(total_o / (R * D) + small_eps)
-    sums_out[...] = jnp.where(lane == 0, scale_q, scale_o)
+    scales_out[...] = jnp.where(lane == 0, scale_q, scale_o)
     for c in done:
         c.sent()
-    for c in (swap_q, swap_o, swap_s):
+    for c in (swap_q, swap_o, swap_s, swap_bq, swap_bo):
         c.wait_send()
-    out.wait()
+    for c in [out] + outs + late:
+        c.wait()
+
+
+def finish(n_hbm, bq_hbm, bo_hbm, wq_hbm, wo_hbm, proj, scales, fq, sq, fo, so,
+           uq, uo, fqn, sqn, fon, son, cq_hbm, co_hbm,
+           n, bq, bo, wq, wo, pq, po, cq, co, sem):
+    fs = lax.axis_index("fs_0") * 4 + lax.axis_index("fs_1")
+    load = lambda src, dst, i: pltpu.make_async_copy(src, dst, sem.at[i])
+    loads = [
+        load(n_hbm, n, 0),
+        load(bq_hbm, bq, 1), load(wq_hbm, wq, 2), load(bo_hbm, bo, 3), load(wo_hbm, wo, 4),
+    ]
+    for c in loads:
+        c.start()
+    fqn[...], sqn[...], _ = moments(fq[...], sq[...], proj[:, 0:512])
+    fon[...], son[...], _ = moments(fo[...], so[...], proj[:, 512:2560])
+    scale_q = scales[0:1, 0:1]
+    scale_o = scales[0:1, 1:2]
+    outs = []
+    loads[0].wait()
+    loads[1].wait()
+    loads[2].wait()
+    for t in range(4):
+        r = slice(t * 256, t * 256 + 256)
+        acc = scale_q * jnp.dot(bq[r, :], n[:, 0:512], preferred_element_type=F32)
+        pq[r, :] = acc
+        cq[r, :] = (wq[r, :].astype(F32) - step_rate * acc).astype(BF)
+        outs.append(load(cq.at[r], cq_hbm.at[r], 5 + t))
+        outs[-1].start()
+    uq[...] = pq[pl.ds(pl.multiple_of(fs * 64, 64), 64), :]
+    loads[3].wait()
+    loads[4].wait()
+    for t in range(4):
+        c = slice(t * 512, t * 512 + 512)
+        acc = scale_o * jnp.dot(bo[...], n[:, 512 + t * 512:1024 + t * 512], preferred_element_type=F32)
+        po[:, c] = acc
+        co[:, c] = (wo[:, c].astype(F32) - step_rate * acc).astype(BF)
+        outs.append(load(co.at[:, c], co_hbm.at[:, c], 9 + t))
+        outs[-1].start()
+    uo[...] = po[pl.ds(pl.multiple_of(fs * 32, 32), 32), :]
+    for c in outs:
+        c.wait()
 
 
 def scratch_for_reduce():
@@ -351,55 +427,68 @@
     return shapes
 
 
-def gathered_moments(x, cq, br, co, bq, bo, fq, sq, fo, so):
+def gathered_moments(*args):
     sds = jax.ShapeDtypeStruct
     dma = pltpu.SemaphoreType.DMA
     return pl.pallas_call(
         kernel,
         out_shape=(
-            sds((8, 512), F32), sds((8, 512), F32), sds((8, 2048), F32), sds((8, 2048), F32),
-            sds((4, 4, 4, 8, WIDE), BF), sds((8, 128), F32),
+            sds((8, 2560), F32), sds((8, 128), F32), sds((4, 4, 4, 8, WIDE), BF),
+            sds((4, 4, 64, 512), BF), sds((4, 4, 32, 512), BF), sds((4, 4, 64, 512), BF), sds((4, 4, 32, 2048), BF),
         ),
-        in_specs=[ANY] * 6 + [VMEM] * 4,
-        out_specs=(VMEM, VMEM, VMEM, VMEM, ANY, VMEM),
+        in_specs=[ANY] * 6 + [VMEM] * 6,
+        out_specs=(VMEM, VMEM, ANY, ANY, ANY, ANY, ANY),
         scratch_shapes=[
             pltpu.VMEM((1024, 4096), BF), pltpu.VMEM((1024, 2048), BF),
             pltpu.VMEM((1024, 512), BF), pltpu.VMEM((1024, 2048), BF),
             pltpu.VMEM((4, 4, 4, 64, 256), BF), pltpu.VMEM((4, 4, 4, 32, 256), BF),
+            pltpu.VMEM((4, 4, 64, 256), BF), pltpu.VMEM((4, 4, 32, 256), BF),
+            pltpu.VMEM((4, 4, 64, 512), BF), pltpu.VMEM((4, 4, 32, 2048), BF),
             pltpu.VMEM((2, 256, 1024), BF), pltpu.VMEM((2, 256, 1024), BF),
             pltpu.VMEM((4, 4, 4, 8, WIDE), BF), pltpu.VMEM((4, 4, 4, 8, WIDE), BF),
-            pltpu.VMEM((8, 2560), F32), pltpu.VMEM((8, 128), F32), pltpu.VMEM((8, 128), F32),
+            pltpu.VMEM((8, 128), F32), pltpu.VMEM((8, 128), F32),
             *scratch_for_reduce(),
-            dma((7,)), dma((54,)), dma((54,)), dma((54,)), dma((54,)), dma((54,)), dma((54,)),
-            dma((3,)), dma((3,)),
+            dma((13,)), dma((54,)), dma((54,)), dma((54,)), dma((54,)), dma((54,)), dma((54,)),
+            dma((36,)), dma((36,)), dma((5,)), dma((5,)),
         ],
         compiler_params=pltpu.CompilerParams(
             collective_id=0, has_side_effects=True, vmem_limit_bytes=60 * 1024 * 1024),
         name="moments_everywhere",
-    )(x, cq, br, co, bq, bo, fq, sq, fo, so)
-
-
-def gather_together(arrays, axis):
-    ravelled = jnp.concatenate([a.reshape(-1) for a in arrays])
-    lines, at, gathered = (lax.all_gather(ravelled, axis), 0, [])
-    for a in arrays:
-        tiles = lines[:, at : at + a.size].reshape(-1, a.shape[1])
-        gathered.append(tiles)
-        at += a.size
-    return tuple(gathered)
+    )(*args)
+
+
+def updates(*args):
+    sds = jax.ShapeDtypeStruct
+    return pl.pallas_call(
+        finish,
+        out_shape=(
+            sds((64, 512), F32), sds((32, 2048), F32),
+            sds((8, 512), F32), sds((8, 512), F32), sds((8, 2048), F32), sds((8, 2048), F32),
+            sds((1024, 512), BF), sds((512, 2048), BF),
+        ),
+        in_specs=[ANY] * 5 + [VMEM] * 6,
+        out_specs=(VMEM,) * 6 + (ANY, ANY),
+        scratch_shapes=[
+            pltpu.VMEM((R, WIDE), BF), pltpu.VMEM((1024, 512), BF), pltpu.VMEM((512, 512), BF),
+            pltpu.VMEM((1024, 512), BF), pltpu.VMEM((512, 2048), BF),
+            pltpu.VMEM((1024, 512), F32), pltpu.VMEM((512, 2048), F32),
+            pltpu.VMEM((1024, 512), BF), pltpu.VMEM((512, 2048), BF),
+            pltpu.SemaphoreType.DMA((13,)),
+        ],
+        compiler_params=pltpu.CompilerParams(vmem_limit_bytes=60 * 1024 * 1024),
+        name="updates",
+    )(*args)
 
 
 def body(query_input, query_cotangent, branch_output, layer_cotangent, query_weight, output_weight,
          query_basis, output_basis, query_first, query_second, output_first, output_second):
-    first_q, second_q, first_o, second_o, normed, scales = gathered_moments(
+    state = (query_first, query_second, output_first, output_second)
+    proj, scales, normed, bq, bo, wq, wo = gathered_moments(
         query_input, query_cotangent, branch_output, layer_cotangent, query_basis, output_basis,
-        query_first, query_second, output_first, output_second)
-    rows = normed.reshape(R, WIDE)
-    update_q = scales[0, 0] * jnp.dot(query_basis, rows[:, 0:512], preferred_element_type=F32)
-    update_o = scales[0, 1] * jnp.dot(output_basis, rows[:, 512:2560], preferred_element_type=F32)
-    query_copy, output_copy = gather_together(
-        ((query_weight - step_rate * update_q).astype(BF), (output_weight - step_rate * update_o).astype(BF)), FS)
-    return (update_q, update_o, first_q, second_q, first_o, second_o, query_copy, output_copy)
+        query_weight, output_weight, *state)
+    return updates(
+        normed.reshape(R, WIDE), bq.reshape(1024, 512), bo.reshape(512, 512), wq.reshape(1024, 512),
+        wo.reshape(512, 2048), proj, scales, *state)
 
 
 def solution(mesh):

time: 172 us -> 110 us (0.64)
  waiting for transfers between devices: 44.1 us -> 0 us
  Pallas kernels: 94.7 us -> 109 us
  local copies, waits for them, and re-layouts: 13.7 us -> 0 us
  between operations: 14.2 us -> 0.64 us
  matrix products: 4.64 us -> 0 us
    all_gather x1 -> x0, waiting for transfers between devices: 44.1 us -> none  [gather_together(): lines, at, gathered = (lax.all_gather(ravelled, axis), 0, [])]
    pallas_call x1 -> x2, Pallas kernels: 94.7 us -> 109 us  [the longest x1 102 us: gathered_moments(): pl.pallas_call(kernel, out_shape=(sds((8, 2560), F32), sds((8, 128), F32)...]
    dot_general x2 -> x0, matrix products: 4.64 us -> none  [the longest x1 2.75 us: body(): jnp.dot(output_basis, rows[:, 512:2560], preferred_element_type=F32)]
    reshape x2 -> x0, local copies, waits for them, and re-layouts: 4.54 us -> none  [gather_together(): tiles = lines[:, at:at + a.size].reshape(-1, a.shape[1])]
    slice x3 -> x0, local copies, waits for them, and re-layouts: 3.84 us -> none  [the longest x2 2.51 us: gather_together(): tiles = lines[:, at:at + a.size].reshape(-1, a.shape[1])]
    all_gather x1 -> x0, local copies, waits for them, and re-layouts: 2.76 us -> none  [gather_together(): lines, at, gathered = (lax.all_gather(ravelled, axis), 0, [])]
    unnamed x28 -> x0, local copies, waits for them, and re-layouts: 2.58 us -> none
  transfers between devices with their start and end apart: 1 -> 0, of which waited for: 1 -> 0; matrix products, arithmetic and copies ran while one was open for 0% -> 0% of each run, Pallas kernels for 0% -> 0%
where the time goes in v2:
time: 110 us
  Pallas kernels  109 us (99%)
    pallas_call x1, Pallas kernels, gathered_moments(): pl.pallas_call(kernel, out_shape=(sds((8, 2560), F32), sds((8, 128), F32)...  102 us
    pallas_call x1, Pallas kernels, updates(): pl.pallas_call(finish, out_shape=(sds((64, 512), F32), sds((32, 2048), F3...  7.21 us

profile of v2, /device:TPU:1, one launch (start us, length us, event | category | flops | bytes accessed | tf_op | source)
XLA Modules:
  0.0 109.7 jit_solution(6060688494792993486)
XLA Ops:
  0.6 101.9 %moments_everywhere.1 = (f32[8,2560]{1,0:T(8,128)}, f32[8,128]{1,0:T(8,128)}, bf16[4,4,4,8,2688]{4,3,2,1,0:T(8,128)(2,1)}, bf16[4,4,64,512]{3,2,1,0:T(8,128)(2,1...) custom-call(bf16[1024,4096]{1,0:T(8,128)(2,1)} %refs_0_.1, ...), custom_call_target="tpu_custom_call" | custom-call | tf_op jit(solution)/shard_map/moments_everywhere/pallas_call | solution.py:433
  102.5 7.2 %updates.1 = (f32[64,512]{1,0:T(8,128)}, f32[32,2048]{1,0:T(8,128)}, f32[8,512]{1,0:T(8,128)}, f32[8,512]{1,0:T(8,128)}, f32[8,2048]{1,0:T(8,128)}, /*index=5*/f...) custom-call(bf16[512,2688]{1,0:T(8,128)(2,1)} %bitcast.5, bf16[1024,512]{1,0:T(8,128)(2,1)} %bitcast.7, ...), custom_call_target="tpu_custom_call" | custom-call | tf_op jit(solution)/shard_map/updates/pallas_call | solution.py:462
